TPU v7x, 32 devices: a whole 2x2x4 slice. The times are simulated.
32 devices in a mesh: sp: 16 (over z, y, x), tp: 2 (over core).
Axes of the slice: x: 2, y: 2, z: 4, core: 2. Of those that a mesh axis runs over, the one named last changes fastest.
Arguments:
- latent: bfloat16 [4096, 2048], P(('sp', 'tp')), may hold values from -6 to 6
- condition: bfloat16 [2048], P('sp'), may hold values from -6 to 6
- context_condition: bfloat16 [2048], P('sp'), may hold values from -6 to 6
- context: bfloat16 [512, 2048], P('sp'), may hold values from -6 to 6
- w_shift: bfloat16 [2048, 2048], P('sp', 'tp'), may hold values from -0.125 to 0.125
- w_scale: bfloat16 [2048, 2048], P('sp', 'tp'), may hold values from -0.125 to 0.125
- w_gate: bfloat16 [2048, 2048], P('sp', 'tp'), may hold values from -0.125 to 0.125
- pre_gain: float32 [2048], replicated, may hold values from 0.1 to 1.9
- post_gain: float32 [2048], replicated, may hold values from 0.1 to 1.9
- query_gain: float32 [128], replicated, may hold values from 0.1 to 5
- key_gain: float32 [128], replicated, may hold values from 0.1 to 5
- w_query: bfloat16 [2048, 2048], P(None, 'tp'), may hold values from -0.125 to 0.125
- w_key: bfloat16 [2048, 1024], P(None, 'tp'), may hold values from -0.125 to 0.125
- w_value: bfloat16 [2048, 1024], P(None, 'tp'), may hold values from -0.125 to 0.125
- w_out: bfloat16 [2048, 2048], P('tp'), may hold values from -0.125 to 0.125
Outputs:
- updated: bfloat16 [4096, 2048], P(('sp', 'tp'))
All inputs are finite; a program needn't handle non-finite values.
Results may differ from a plain program's by a relative error of at most 0.0085.
The roundings to bfloat16 on the way count: a program that leaves them out, or rounds other values in their place, can miss the bound.
Values may be sent and summed in bfloat16 or wider, within the bound.
A program may use at most 64 MiB of HBM per device.

v0:
```python
import functools
import math

import jax
import jax.numpy as jnp
from jax import lax
from jax.experimental import pallas as pl
from jax.experimental.pallas import tpu as pltpu
from jax.sharding import PartitionSpec as P

GRID_W = 64
EPS = 1e-06
F32 = jnp.float32
BF16 = jnp.bfloat16
MESH = pl.DeviceIdType.MESH


def kernel(
    sizes,
    latent,
    cond,
    ctx_cond,
    context,
    w_shift,
    w_scale,
    w_gate,
    pre_gain,
    post_gain,
    query_gain,
    key_gain,
    w_query,
    w_key,
    w_value,
    w_out,
    out,
    wq,
    wkv,
    wo,
    lat_all,
    mod_part,
    mod_recv,
    gate_part,
    gate_recv,
    mod_all,
    gate_all,
    xn,
    kv_send,
    cx_send,
    q_send,
    kvb,
    cxb,
    qb,
    m_ref,
    l_ref,
    acc_ref,
    att_send,
    att_recv,
    part_send,
    part_recv,
    w_sem,
    lat_ss,
    lat_rs,
    mp_ss,
    mp_rs,
    gp_ss,
    gp_rs,
    ma_ss,
    ma_rs,
    ga_ss,
    ga_rs,
    kva_ss,
    cxa_ss,
    kvz_ss,
    cxz_ss,
    kv_rs,
    cx_rs,
    q_ss,
    q_rs,
    at_ss,
    at_rs,
    pt_ss,
    pt_rs,
):
    n_sp, n_tp, fan, planes, group, hd, tok, rows, ctx = sizes
    width = w_shift.shape[1]
    depth = latent.shape[1]
    qw = group * hd
    me = lax.axis_index("sp")
    mt = lax.axis_index("tp")
    if fan == 1:
        f, g = 0, me
    else:
        f, g = lax.rem(me, fan), lax.div(me, fan)

    def remote(src, dst, ss, rs, **where):
        return pltpu.make_async_remote_copy(
            src_ref=src, dst_ref=dst, send_sem=ss, recv_sem=rs, device_id=where, device_id_type=MESH
        )

    loads = [pltpu.make_async_copy(w_query, wq, w_sem.at[0])]
    kv_loads = []
    for i in range(fan):
        cols = pl.ds(i * hd, hd)
        kv_loads.append(
            pltpu.make_async_copy(w_key.at[:, cols], wkv.at[i, :, pl.ds(0, hd)], w_sem.at[2 + 2 * i])
        )
        kv_loads.append(
            pltpu.make_async_copy(
                w_value.at[:, cols], wkv.at[i, :, pl.ds(hd, hd)], w_sem.at[3 + 2 * i]
            )
        )
    out_load = pltpu.make_async_copy(w_out, wo, w_sem.at[1])
    for copy in kv_loads + loads + [out_load]:
        copy.start()

    bar = pltpu.get_barrier_semaphore()

    @pl.loop(1, n_sp)
    def _(d):
        pl.semaphore_signal(
            bar, inc=1, device_id={"sp": lax.rem(me + d, n_sp)}, device_id_type=MESH
        )

    for d in range(1, n_tp):
        pl.semaphore_signal(
            bar, inc=1, device_id={"tp": lax.rem(mt + d, n_tp)}, device_id_type=MESH
        )

    def silu(v):
        v = v.astype(F32)
        return v / (1.0 + jnp.exp(-v))

    row_id = lax.broadcasted_iota(jnp.int32, (8, cond.shape[1]), 0)
    conds = jnp.where(
        row_id == 0, silu(cond[...]), jnp.where(row_id == 1, silu(ctx_cond[...]), 0.0)
    ).astype(BF16)
    part_shift = jnp.dot(conds, w_shift[...], preferred_element_type=F32)
    part_scale = jnp.dot(conds, w_scale[...], preferred_element_type=F32)
    part_gate = jnp.dot(conds, w_gate[...], preferred_element_type=F32)
    mod_part[0:2, :] = part_shift[0:2]
    mod_part[2:4, :] = part_scale[0:2]
    gate_part[...] = part_gate[0:1]
    pl.semaphore_wait(bar, n_sp - 1 + n_tp - 1)

    def mod_copy(d, slot):
        peer = lax.rem(me + d, n_sp)
        return remote(mod_part, mod_recv.at[slot], mp_ss.at[d], mp_rs.at[slot], sp=peer)

    def gate_copy(d, slot):
        peer = lax.rem(me + d, n_sp)
        return remote(gate_part, gate_recv.at[slot], gp_ss.at[d], gp_rs.at[slot], sp=peer)

    @pl.loop(1, n_sp)
    def _(d):
        mod_copy(d, me).start()

    def lat_copy(d, slot):
        peer = lax.rem(mt + d, n_tp)
        return remote(latent, lat_all.at[slot], lat_ss.at[d], lat_rs.at[slot], tp=peer)

    for d in range(1, n_tp):
        lat_copy(d, mt).start()

    @pl.loop(1, n_sp)
    def _(d):
        gate_copy(d, me).start()

    mod_recv[me] = mod_part[...]
    gate_recv[me] = gate_part[...]
    lat_all[mt] = latent[...]

    lane = lax.broadcasted_iota(jnp.int32, (tok, hd), 1)
    quarter = hd // 4
    pos = (me * tok + lax.broadcasted_iota(jnp.int32, (tok, hd), 0)).astype(F32)
    row_pos = jnp.floor(pos * (1.0 / GRID_W))
    col_pos = pos - row_pos * GRID_W
    step = (lane & (quarter - 1)).astype(F32)
    freq = jnp.exp(step * (-2.0 * math.log(10000.0) / (hd // 2)))
    angle = jnp.where(lane < hd // 2, row_pos, col_pos) * freq
    low = (lane & quarter) == 0
    cosine = jnp.cos(angle)
    sine = jnp.sin(angle)
    sine = jnp.where(low, -sine, sine)

    def head_rms(v, gain):
        return v * lax.rsqrt(jnp.mean(v * v, axis=-1, keepdims=True) + EPS) * gain

    def rotate(v):
        other = jnp.where(low, pltpu.roll(v, hd - quarter, 1), pltpu.roll(v, quarter, 1))
        return v * cosine + other * sine

    for d in range(1, n_tp):
        lat_copy(d, lax.rem(mt + d, n_tp)).wait_recv()

    def inverse(v):
        return lax.rsqrt(jnp.mean(v * v, axis=-1, keepdims=True) + EPS)

    lat_inv = [inverse(lat_all[t].astype(F32)) for t in range(n_tp)]
    ctx_inv = inverse(context[...].astype(F32))

    @pl.loop(1, n_sp)
    def _(d):
        mod_copy(d, lax.rem(me + d, n_sp)).wait_recv()

    total = lax.fori_loop(
        1, n_sp, lambda i, s: s + mod_recv[i], mod_recv[0]
    )
    mod_all[mt] = total

    def ma_copy(d, slot):
        peer = lax.rem(mt + d, n_tp)
        return remote(mod_all.at[mt], mod_all.at[slot], ma_ss.at[d], ma_rs.at[slot], tp=peer)

    for d in range(1, n_tp):
        ma_copy(d, mt).start()
    for d in range(1, n_tp):
        ma_copy(d, lax.rem(mt + d, n_tp)).wait_recv()

    for t in range(n_tp):
        cols = slice(t * width, (t + 1) * width)
        shift0, shift1 = mod_all[t, 0:1], mod_all[t, 1:2]
        scale0, scale1 = mod_all[t, 2:3], mod_all[t, 3:4]
        gain = pre_gain[:, cols]
        for s in range(n_tp):
            v = lat_all[s, :, cols].astype(F32) * lat_inv[s] * gain
            xn[s * rows : (s + 1) * rows, cols] = (v * (1.0 + scale0) + shift0).astype(BF16)
        v = context[:, cols].astype(F32) * ctx_inv * gain
        xn[tok : tok + ctx, cols] = (v * (1.0 + scale1) + shift1).astype(BF16)

    for copy in kv_loads:
        copy.wait()
    mine = pl.ds(pl.multiple_of(f * tok, tok), tok) if fan > 1 else pl.ds(0, tok)
    mine_c = pl.ds(pl.multiple_of(f * ctx, ctx), ctx) if fan > 1 else pl.ds(0, ctx)

    def block_rows(i):
        if fan == 1:
            return pl.ds(0, tok), pl.ds(0, ctx)
        return (
            pl.ds(pl.multiple_of(i * tok, tok), tok),
            pl.ds(pl.multiple_of(i * ctx, ctx), ctx),
        )

    def chip(plane, i):
        return plane * fan + i

    def project_kv(i):
        both = jnp.dot(xn[...], wkv[i], preferred_element_type=F32)
        k = head_rms(both[:, :hd], key_gain[...])
        v = both[:, hd:].astype(BF16)
        key = rotate(k[:tok]).astype(BF16)
        return key, v[:tok], k[tok:].astype(BF16), v[tok:]

    def kva_copy(i):
        return remote(
            kv_send.at[i], kvb.at[g, :, mine], kva_ss.at[i], kv_rs.at[me], sp=chip(g, i)
        )

    def cxa_copy(i):
        return remote(
            cx_send.at[i], cxb.at[g, :, mine_c], cxa_ss.at[i], cx_rs.at[me], sp=chip(g, i)
        )

    def kvz_copy(way, plane, i):
        r, rc = block_rows(i)
        src = chip(plane, i)
        peer = me + fan if way == 0 else me - fan
        return remote(
            kvb.at[plane, :, r], kvb.at[plane, :, r], kvz_ss.at[way, src], kv_rs.at[src], sp=peer
        )

    def cxz_copy(way, plane, i):
        r, rc = block_rows(i)
        src = chip(plane, i)
        peer = me + fan if way == 0 else me - fan
        return remote(
            cxb.at[plane, :, rc], cxb.at[plane, :, rc], cxz_ss.at[way, src], cx_rs.at[src], sp=peer
        )

    def pass_on(way, plane, i):
        room = g < planes - 1 if way == 0 else g > 0

        @pl.when(room)
        def _():
            kvz_copy(way, plane, i).start()
            cxz_copy(way, plane, i).start()

    def block_wait(plane, i):
        kvz_copy(0, plane, i).wait_recv()
        cxz_copy(0, plane, i).wait_recv()

    key, val, ckey, cval = project_kv(f)
    kvb[g, 0, mine] = key
    kvb[g, 1, mine] = val
    cxb[g, 0, mine_c] = ckey
    cxb[g, 1, mine_c] = cval
    pass_on(0, g, f)
    pass_on(1, g, f)
    for d in range(1, fan):
        i = lax.rem(f + d, fan)
        key, val, ckey, cval = project_kv(i)
        kv_send[i, 0] = key
        kv_send[i, 1] = val
        cx_send[i, 0] = ckey
        cx_send[i, 1] = cval
        kva_copy(i).start()
        cxa_copy(i).start()

    for copy in loads:
        copy.wait()

    def project_q(i):
        if fan == 1:
            w = wq[...]
        else:
            w = wq[:, pl.ds(pl.multiple_of(i * qw, qw), qw)]
        q = jnp.dot(xn[0:tok], w, preferred_element_type=F32)
        return [
            rotate(head_rms(q[:, h * hd : (h + 1) * hd], query_gain[...])).astype(BF16)
            for h in range(group)
        ]

    def q_copy(i, slot):
        return remote(q_send.at[i], qb.at[slot], q_ss.at[i], q_rs.at[slot], sp=chip(g, i))

    for d in range(1, fan):
        i = lax.rem(f + d, fan)
        for h, q in enumerate(project_q(i)):
            q_send[i, h] = q
        q_copy(i, f).start()
        j = lax.rem(f + fan - d, fan)
        block_wait(g, j)
        pass_on(0, g, j)
        pass_on(1, g, j)
    for h, q in enumerate(project_q(f)):
        qb[f, h] = q
    m_ref[...] = jnp.full(m_ref.shape, -1e30, F32)
    l_ref[...] = jnp.zeros(l_ref.shape, F32)
    acc_ref[...] = jnp.zeros(acc_ref.shape, F32)
    root = math.sqrt(hd)
    lift = math.log(tok * n_sp / (4.0 * ctx * n_sp)) * root
    factor = math.log2(math.e) / root
    contract = (((1,), (1,)), ((), ()))

    def absorb(i, key, value, ckey, cvalue):
        for h in range(group):
            q = qb[i, h]
            s = lax.dot_general(q, key, contract, preferred_element_type=F32)
            c = lax.dot_general(q, ckey, contract, preferred_element_type=F32) + lift
            old = m_ref[i, h]
            new = jnp.maximum(
                jnp.maximum(old, jnp.max(s, axis=-1, keepdims=True)),
                jnp.max(c, axis=-1, keepdims=True),
            )
            fade = jnp.exp2((old - new) * factor)
            s = jnp.exp2((s - new) * factor)
            c = jnp.exp2((c - new) * factor)
            m_ref[i, h] = new
            l_ref[i, h] = (
                l_ref[i, h] * fade
                + jnp.sum(s, axis=-1, keepdims=True)
                + jnp.sum(c, axis=-1, keepdims=True)
            )
            acc_ref[i, h] = (
                acc_ref[i, h] * fade
                + jnp.dot(s.astype(BF16), value, preferred_element_type=F32)
                + jnp.dot(c.astype(BF16), cvalue, preferred_element_type=F32)
            )

    def before(n):
        return lax.rem(f + fan - n, fan) if fan > 1 else 0

    def attend(plane, hook):
        @pl.loop(0, fan)
        def _(n):
            hook(n)
            absorb(before(n), kvb[plane, 0], kvb[plane, 1], cxb[plane, 0], cxb[plane, 1])

    def at_copy(i, slot):
        return remote(
            att_send.at[i], att_recv.at[slot], at_ss.at[i], at_rs.at[slot], sp=chip(g, i)
        )

    def attended(i):
        return [(acc_ref[i, h] / l_ref[i, h]).astype(BF16) for h in range(group)]

    def give(n, i):
        @pl.when(n < fan - 1)
        def _():
            for h, a in enumerate(attended(i)):
                att_send[i, :, h * hd : (h + 1) * hd] = a
            at_copy(i, f).start()

        @pl.when(n == fan - 1)
        def _():
            for h, a in enumerate(attended(f)):
                att_recv[f, :, h * hd : (h + 1) * hd] = a

    def after(n):
        return lax.rem(f + 1 + n, fan) if fan > 1 else 0

    top, bottom = g == planes - 1, g == 0
    edge = top | bottom

    def arrive(t, n):
        i = before(n)

        @pl.when((g - t >= 0) & (g < planes - 1))
        def _():
            block_wait(g - t, i)
            pass_on(0, g - t, i)

        @pl.when((g + t < planes) & (g > 0))
        def _():
            block_wait(g + t, i)
            pass_on(1, g + t, i)

    def first_hook(n):
        if fan > 1:

            @pl.when(n > 0)
            def _():
                q_copy(f, before(n)).wait_recv()

        arrive(1, n)

    attend(g, first_hook)

    @pl.loop(1, planes - 1)
    def _(t):
        for n in range(fan):

            @pl.when(top)
            def _():
                block_wait(g - t, before(n))

            @pl.when(bottom)
            def _():
                block_wait(g + t, before(n))

        @pl.when(g - t >= 0)
        def _():
            attend(g - t, lambda n: arrive(t + 1, n))

        @pl.when((g + t < planes) & (g - t < 0))
        def _():
            attend(g + t, lambda n: arrive(t + 1, n))

        @pl.when((g + t < planes) & (g - t >= 0))
        def _():
            attend(g + t, lambda n: None)

    @pl.when(edge)
    def _():
        far = jnp.where(bottom, planes - 1, 0)

        @pl.loop(0, fan)
        def _(d):
            j = before(d)
            r, rc = block_rows(j)
            block_wait(far, j)

            @pl.loop(0, fan)
            def _(n):
                i = after(n)
                absorb(i, kvb[far, 0, r], kvb[far, 1, r], cxb[far, 0, rc], cxb[far, 1, rc])

                @pl.when(d == fan - 1)
                def _():
                    give(n, i)

    @pl.when(jnp.logical_not(edge))
    def _():
        @pl.loop(0, fan)
        def _(n):
            give(n, after(n))

    @pl.loop(1, n_sp)
    def _(d):
        gate_copy(d, lax.rem(me + d, n_sp)).wait_recv()

    gate_all[mt] = lax.fori_loop(1, n_sp, lambda i, s: s + gate_recv[i], gate_recv[0])

    def ga_copy(d, slot):
        peer = lax.rem(mt + d, n_tp)
        return remote(gate_all.at[mt], gate_all.at[slot], ga_ss.at[d], ga_rs.at[slot], tp=peer)

    for d in range(1, n_tp):
        ga_copy(d, mt).start()
    out_load.wait()
    for d in range(1, fan):
        at_copy(f, lax.rem(f + d, fan)).wait_recv()

    def project_out(t):
        r = pl.ds(pl.multiple_of(t * rows, rows), rows)
        wide = jnp.concatenate([att_recv[i, r] for i in range(fan)], axis=-1)
        return jnp.dot(wide, wo[...], preferred_element_type=F32).astype(BF16)

    def pt_copy(d, t, slot):
        return remote(part_send.at[t], part_recv.at[slot], pt_ss.at[t], pt_rs.at[slot], tp=t)

    for d in range(1, n_tp):
        t = lax.rem(mt + d, n_tp)
        part_send[t] = project_out(t)
        pt_copy(d, t, mt).start()
    part_recv[mt] = project_out(mt)
    for d in range(1, n_tp):
        ga_copy(d, lax.rem(mt + d, n_tp)).wait_recv()
    for d in range(1, n_tp):
        t = lax.rem(mt + d, n_tp)
        pt_copy(d, t, t).wait_recv()
    mixed = part_recv[0].astype(F32)
    for t in range(1, n_tp):
        mixed = mixed + part_recv[t].astype(F32)
    inv = lax.rsqrt(jnp.mean(mixed * mixed, axis=-1, keepdims=True) + EPS)
    for t in range(n_tp):
        cols = slice(t * width, (t + 1) * width)
        out[:, cols] = (
            latent[:, cols].astype(F32)
            + gate_all[t] * (mixed[:, cols] * inv * post_gain[:, cols])
        ).astype(BF16)

    @pl.loop(1, n_sp)
    def _(d):
        mod_copy(d, me).wait_send()
        gate_copy(d, me).wait_send()

    for d in range(1, n_tp):
        lat_copy(d, mt).wait_send()
        ma_copy(d, mt).wait_send()
        ga_copy(d, mt).wait_send()
        t = lax.rem(mt + d, n_tp)
        pt_copy(d, t, mt).wait_send()
    for d in range(1, fan):
        i = lax.rem(f + d, fan)
        kva_copy(i).wait_send()
        cxa_copy(i).wait_send()
        q_copy(i, f).wait_send()
        at_copy(i, f).wait_send()

    @pl.loop(0, planes)
    def _(plane):
        for i in range(fan):

            @pl.when((plane <= g) & (g < planes - 1))
            def _():
                kvz_copy(0, plane, i).wait_send()
                cxz_copy(0, plane, i).wait_send()

            @pl.when((plane >= g) & (g > 0))
            def _():
                kvz_copy(1, plane, i).wait_send()
                cxz_copy(1, plane, i).wait_send()


def body(
    latent,
    condition,
    context_condition,
    context,
    w_shift,
    w_scale,
    w_gate,
    pre_gain,
    post_gain,
    query_gain,
    key_gain,
    w_query,
    w_key,
    w_value,
    w_out,
):
    n_sp = lax.axis_size("sp")
    n_tp = lax.axis_size("tp")
    hd = query_gain.shape[0]
    kv_dev = w_key.shape[1] // hd
    group = w_query.shape[1] // w_key.shape[1]
    fan = kv_dev
    planes = n_sp // fan
    rows, depth = latent.shape
    tok = rows * n_tp
    ctx = context.shape[0]
    width = w_shift.shape[1]
    sizes = (n_sp, n_tp, fan, planes, group, hd, tok, rows, ctx)
    vmem = pl.BlockSpec(memory_space=pltpu.VMEM)
    hbm = pl.BlockSpec(memory_space=pl.ANY)
    dma = pltpu.SemaphoreType.DMA
    scratch = [
        pltpu.VMEM(w_query.shape, BF16),
        pltpu.VMEM((fan, depth, 2 * hd), BF16),
        pltpu.VMEM(w_out.shape, BF16),
        pltpu.VMEM((n_tp, rows, depth), BF16),
        pltpu.VMEM((4, width), F32),
        pltpu.VMEM((n_sp, 4, width), F32),
        pltpu.VMEM((1, width), F32),
        pltpu.VMEM((n_sp, 1, width), F32),
        pltpu.VMEM((n_tp, 4, width), F32),
        pltpu.VMEM((n_tp, 1, width), F32),
        pltpu.VMEM((tok + ctx, depth), BF16),
        pltpu.VMEM((fan, 2, tok, hd), BF16),
        pltpu.VMEM((fan, 2, ctx, hd), BF16),
        pltpu.VMEM((fan, group, tok, hd), BF16),
        pltpu.VMEM((planes, 2, fan * tok, hd), BF16),
        pltpu.VMEM((planes, 2, fan * ctx, hd), BF16),
        pltpu.VMEM((fan, group, tok, hd), BF16),
        pltpu.VMEM((fan, group, tok, 1), F32),
        pltpu.VMEM((fan, group, tok, 1), F32),
        pltpu.VMEM((fan, group, tok, hd), F32),
        pltpu.VMEM((fan, tok, group * hd), BF16),
        pltpu.VMEM((fan, tok, group * hd), BF16),
        pltpu.VMEM((n_tp, rows, depth), BF16),
        pltpu.VMEM((n_tp, rows, depth), BF16),
        dma((2 + 2 * fan,)),
        dma((n_tp,)),
        dma((n_tp,)),
        dma((n_sp,)),
        dma((n_sp,)),
        dma((n_sp,)),
        dma((n_sp,)),
        dma((n_tp,)),
        dma((n_tp,)),
        dma((n_tp,)),
        dma((n_tp,)),
        dma((fan,)),
        dma((fan,)),
        dma((2, n_sp)),
        dma((2, n_sp)),
        dma((n_sp,)),
        dma((n_sp,)),
        dma((fan,)),
        dma((fan,)),
        dma((fan,)),
        dma((fan,)),
        dma((n_tp,)),
        dma((n_tp,)),
    ]
    return pl.pallas_call(
        functools.partial(kernel, sizes),
        out_shape=jax.ShapeDtypeStruct(latent.shape, BF16),
        in_specs=[vmem] * 11 + [hbm] * 4,
        out_specs=vmem,
        scratch_shapes=scratch,
        compiler_params=pltpu.CompilerParams(
            collective_id=0, has_side_effects=True, vmem_limit_bytes=60 * 1024 * 1024
        ),
    )(
        latent,
        condition.reshape(1, -1),
        context_condition.reshape(1, -1),
        context,
        w_shift,
        w_scale,
        w_gate,
        pre_gain.reshape(1, -1),
        post_gain.reshape(1, -1),
        query_gain.reshape(1, -1),
        key_gain.reshape(1, -1),
        w_query,
        w_key,
        w_value,
        w_out,
    )


def solution(mesh):
    placed = (
        P(("sp", "tp"), None),
        P("sp"),
        P("sp"),
        P("sp", None),
        P("sp", "tp"),
        P("sp", "tp"),
        P("sp", "tp"),
        P(),
        P(),
        P(),
        P(),
        P(None, "tp"),
        P(None, "tp"),
        P(None, "tp"),
        P("tp", None),
    )
    return jax.shard_map(
        body, mesh=mesh, in_specs=placed, out_specs=P(("sp", "tp"), None), check_vma=False
    )
```

profile of v0, /device:TPU:1, one launch (start us, length us, event | category | flops | bytes accessed | tf_op | source)
XLA Modules:
  0.0 84.7 jit_solution(2265781392547271535)
XLA Ops:
  0.0 82.8 %shard_map.145 = bf16[128,2048]{1,0:T(8,128)(2,1)} custom-call(bf16[128,2048]{1,0:T(8,128)(2,1)} %latent.1, bf16[1,128]{1,0:T(2,128)(2,1)} %bitcast.8, bf16[1,128]{1,0:T(2,128)(2,1)} %bitcast.9, bf16[32,2048]{1,0:T(8,128)(2,1)} %context.1, bf16[128,1024]{1,0:T(8,128)(2,1)} %w_shift.1, bf16[128,1024]{1,0:T(8,128)(2,1)} %w_scale.1, bf16[128,1024]{1,0:T(8,128)(2,1)} %w_gate.1, ...), custom_call_target="tpu_custom_call" | custom-call | tf_op jit(solution)/shard_map/pallas_call | solution.py:636
  82.8 1.9 %copy.17 = bf16[128,2048]{1,0:T(8,128)(2,1)} copy(bf16[128,2048]{1,0:T(8,128)(2,1)} %shard_map.145) | data formatting | bytes 1048576
where the time goes:
time: 84.9 us; the launch traced here: 84.7 us
  Pallas kernels  82.8 us (98%)
  local copies, waits for them, and re-layouts  1.88 us (2%)
    pallas_call x1, Pallas kernels, body(): pl.pallas_call(functools.partial(kernel, sizes), out_shape=jax.ShapeDtype...  82.8 us
    unnamed x1, local copies, waits for them, and re-layouts  1.88 us

commit v1 on v0

v1 whole, which is shorter than its diff:
```python
import functools
import math

import jax
import jax.numpy as jnp
from jax import lax
from jax.experimental import pallas as pl
from jax.experimental.pallas import tpu as pltpu
from jax.sharding import PartitionSpec as P

GRID_W = 64
EPS = 1e-06
ONES = 16
F32 = jnp.float32
BF16 = jnp.bfloat16
MESH = pl.DeviceIdType.MESH


def kernel(
    sizes,
    latent,
    cond,
    ctx_cond,
    context,
    w_shift,
    w_scale,
    w_gate,
    pre_gain,
    post_gain,
    query_gain,
    key_gain,
    w_query,
    w_key,
    w_value,
    w_out,
    out,
    wq,
    wkv,
    wo,
    lat_all,
    lat_next,
    mod_part,
    mod_recv,
    gate_part,
    gate_recv,
    mod_all,
    gate_all,
    xn,
    kv_send,
    q_send,
    kvb,
    qb,
    m_ref,
    acc_ref,
    s0,
    s1,
    n0,
    n1,
    att_send,
    att_recv,
    psum,
    part_send,
    part_recv,
    w_sem,
    lat_ss,
    lat_rs,
    ln_ss,
    ln_rs,
    lz_ss,
    red_sem,
    ma_ss,
    ma_rs,
    ga_ss,
    ga_rs,
    kva_ss,
    kvz_ss,
    kv_rs,
    cx_ss,
    cx_rs,
    q_ss,
    q_rs,
    at_ss,
    at_rs,
    pt_ss,
    pt_rs,
):
    n_sp, n_tp, fan, planes, group, hd, tok, rows, ctx = sizes
    width = w_shift.shape[1]
    qw = group * hd
    wide = group * tok
    early = planes >= 4
    me = lax.axis_index("sp")
    mt = lax.axis_index("tp")
    if fan == 1:
        f, g = 0, me
    else:
        f, g = lax.rem(me, fan), lax.div(me, fan)
    top, bottom = g == planes - 1, g == 0
    edge = top | bottom
    beside = jnp.where(bottom, 1, planes - 2)

    def remote(src, dst, ss, rs, **where):
        return pltpu.make_async_remote_copy(
            src_ref=src, dst_ref=dst, send_sem=ss, recv_sem=rs, device_id=where, device_id_type=MESH
        )

    loads = [pltpu.make_async_copy(w_query, wq, w_sem.at[0])]
    kv_loads = []
    for i in range(fan):
        cols = pl.ds(i * hd, hd)
        kv_loads.append(
            pltpu.make_async_copy(w_key.at[:, cols], wkv.at[i, :, pl.ds(0, hd)], w_sem.at[2 + 2 * i])
        )
        kv_loads.append(
            pltpu.make_async_copy(
                w_value.at[:, cols], wkv.at[i, :, pl.ds(hd, hd)], w_sem.at[3 + 2 * i]
            )
        )
    out_load = pltpu.make_async_copy(w_out, wo, w_sem.at[1])
    for copy in kv_loads + loads + [out_load]:
        copy.start()

    bar = pltpu.get_barrier_semaphore()

    @pl.loop(1, n_sp)
    def _(d):
        pl.semaphore_signal(
            bar, inc=1, device_id={"sp": lax.rem(me + d, n_sp)}, device_id_type=MESH
        )

    for d in range(1, n_tp):
        pl.semaphore_signal(
            bar, inc=1, device_id={"tp": lax.rem(mt + d, n_tp)}, device_id_type=MESH
        )

    def silu(v):
        v = v.astype(F32)
        return v / (1.0 + jnp.exp(-v))

    row_id = lax.broadcasted_iota(jnp.int32, (8, cond.shape[1]), 0)
    conds = jnp.where(
        row_id == 0, silu(cond[...]), jnp.where(row_id == 1, silu(ctx_cond[...]), 0.0)
    ).astype(BF16)
    part_shift = jnp.dot(conds, w_shift[...], preferred_element_type=F32)
    part_scale = jnp.dot(conds, w_scale[...], preferred_element_type=F32)
    part_gate = jnp.dot(conds, w_gate[...], preferred_element_type=F32)
    mod_part[0:2, :] = part_shift[0:2]
    mod_part[2:4, :] = part_scale[0:2]
    gate_part[...] = part_gate[0:1]

    lane = lax.broadcasted_iota(jnp.int32, (tok, hd), 1)
    quarter = hd // 4
    low = (lane & quarter) == 0

    def turns(chip_index):
        pos = (chip_index * tok + lax.broadcasted_iota(jnp.int32, (tok, hd), 0)).astype(F32)
        row_pos = jnp.floor(pos * (1.0 / GRID_W))
        col_pos = pos - row_pos * GRID_W
        step = (lane & (quarter - 1)).astype(F32)
        freq = jnp.exp(step * (-2.0 * math.log(10000.0) / (hd // 2)))
        angle = jnp.where(lane < hd // 2, row_pos, col_pos) * freq
        sine = jnp.sin(angle)
        return jnp.cos(angle), jnp.where(low, -sine, sine)

    pl.semaphore_wait(bar, n_sp - 1 + n_tp - 1)

    def mod_copy(d, slot):
        peer = lax.rem(me + d, n_sp)
        return remote(mod_part, mod_recv.at[slot], red_sem.at[0], red_sem.at[1], sp=peer)

    def gate_copy(d, slot):
        peer = lax.rem(me + d, n_sp)
        return remote(gate_part, gate_recv.at[slot], red_sem.at[2], red_sem.at[3], sp=peer)

    def wait_all(ref, sem):
        most = ref.at[pl.ds(0, n_sp - 1)]
        pltpu.make_async_copy(most, most, sem).wait()

    @pl.loop(1, n_sp)
    def _(d):
        mod_copy(d, d - 1).start()

    def lat_copy(d, slot):
        peer = lax.rem(mt + d, n_tp)
        return remote(latent, lat_all.at[slot], lat_ss.at[d], lat_rs.at[slot], tp=peer)

    for d in range(1, n_tp):
        lat_copy(d, mt).start()

    @pl.loop(1, n_sp)
    def _(d):
        gate_copy(d, d - 1).start()

    def next_copy(way):
        peer = me + fan if way == 0 else me - fan
        return remote(latent, lat_next.at[mt], lz_ss.at[way], ln_rs.at[mt], sp=peer)

    send_up = early & (g == planes - 2)
    send_down = early & (g == 1)

    @pl.when(send_up)
    def _():
        next_copy(0).start()

    @pl.when(send_down)
    def _():
        next_copy(1).start()

    mod_recv[n_sp - 1] = mod_part[...]
    gate_recv[n_sp - 1] = gate_part[...]
    lat_all[mt] = latent[...]

    cosine, sine = turns(me)

    def head_rms(v, gain):
        return v * lax.rsqrt(jnp.mean(v * v, axis=-1, keepdims=True) + EPS) * gain

    def rotate(v, cosine, sine):
        other = jnp.where(low, pltpu.roll(v, hd - quarter, 1), pltpu.roll(v, quarter, 1))
        return v * cosine + other * sine

    for d in range(1, n_tp):
        lat_copy(d, lax.rem(mt + d, n_tp)).wait_recv()

    def inverse(v):
        return lax.rsqrt(jnp.mean(v * v, axis=-1, keepdims=True) + EPS)

    lat_inv = [inverse(lat_all[t].astype(F32)) for t in range(n_tp)]
    ctx_inv = inverse(context[...].astype(F32))
    m_ref[...] = jnp.full(m_ref.shape, -1e30, F32)
    acc_ref[...] = jnp.zeros(acc_ref.shape, F32)

    wait_all(mod_recv, red_sem.at[1])
    mod_all[mt] = lax.fori_loop(1, n_sp, lambda i, s: s + mod_recv[i], mod_recv[0])

    def ma_copy(d, slot):
        peer = lax.rem(mt + d, n_tp)
        return remote(mod_all.at[mt], mod_all.at[slot], ma_ss.at[d], ma_rs.at[slot], tp=peer)

    for d in range(1, n_tp):
        ma_copy(d, mt).start()
    for d in range(1, n_tp):
        ma_copy(d, lax.rem(mt + d, n_tp)).wait_recv()

    def modulate(latents, inverses):
        for t in range(n_tp):
            cols = slice(t * width, (t + 1) * width)
            scale0 = 1.0 + mod_all[t, 2:3]
            for s in range(n_tp):
                v = latents[s, :, cols].astype(F32) * inverses[s] * pre_gain[:, cols]
                xn[s * rows : (s + 1) * rows, cols] = (v * scale0 + mod_all[t, 0:1]).astype(BF16)

    modulate(lat_all, lat_inv)
    for t in range(n_tp):
        cols = slice(t * width, (t + 1) * width)
        v = context[:, cols].astype(F32) * ctx_inv * pre_gain[:, cols]
        xn[tok : tok + ctx, cols] = (v * (1.0 + mod_all[t, 3:4]) + mod_all[t, 1:2]).astype(BF16)

    for copy in kv_loads:
        copy.wait()

    def chip(plane, i):
        return plane * fan + i

    main = pl.ds(0, 2 * tok)
    extra = pl.ds(2 * tok, 2 * ctx)

    def put_kv(both, dst, cosine, sine):
        k = head_rms(both[:, :hd], key_gain[...])
        v = both[:, hd:]
        dst[0:tok] = rotate(k[:tok], cosine, sine).astype(BF16)
        for c in range(tok // hd):
            dst[tok + c * hd : tok + (c + 1) * hd] = v[c * hd : (c + 1) * hd].T.astype(BF16)
        if both.shape[0] > tok:
            dst[2 * tok : 2 * tok + ctx] = k[tok:].astype(BF16)
            dst[2 * tok + ctx : 2 * tok + 2 * ctx] = v[tok:].astype(BF16)

    def kva_copy(i):
        return remote(
            kv_send.at[0, i], kvb.at[g, f], kva_ss.at[0, i], kv_rs.at[me], sp=chip(g, i)
        )

    def kvn_copy(i, slot):
        return remote(
            kv_send.at[1, i, main],
            kvb.at[beside, slot, main],
            kva_ss.at[1, i],
            kv_rs.at[chip(beside, slot)],
            sp=chip(g, i),
        )

    def kvz_copy(way, plane, i, slot):
        peer = me + fan if way == 0 else me - fan
        return remote(
            kvb.at[plane, i], kvb.at[plane, i], kvz_ss.at[slot], kv_rs.at[chip(plane, i)], sp=peer
        )

    def cxz_copy(way, i):
        peer = me + fan if way == 0 else me - fan
        return remote(kvb.at[g, i, extra], kvb.at[g, i, extra], cx_ss.at[i], cx_rs.at[i], sp=peer)

    def pass_own(way, i):
        room = g < planes - 1 if way == 0 else g > 0
        short = send_up if way == 0 else send_down

        @pl.when(room & jnp.logical_not(short))
        def _():
            kvz_copy(way, g, i, chip(g, i) if way == 0 else n_sp + i).start()

        @pl.when(short)
        def _():
            cxz_copy(way, i).start()

    def pass_on(way, plane, i):
        kvz_copy(way, plane, i, chip(plane, i)).start()

    def block_wait(plane, i):
        kvz_copy(0, plane, i, 0).wait_recv()

    def project_kv(i, dst):
        put_kv(jnp.dot(xn[...], wkv[i], preferred_element_type=F32), dst, cosine, sine)

    project_kv(f, kvb.at[g, f])
    pass_own(0, f)
    pass_own(1, f)
    for d in range(1, fan):
        i = lax.rem(f + d, fan)
        project_kv(i, kv_send.at[0, i])
        kva_copy(i).start()

    for copy in loads:
        copy.wait()
    factor = math.log2(math.e) / math.sqrt(hd)

    def project_q(i, dst):
        if fan == 1:
            w = wq[...]
        else:
            w = wq[:, pl.ds(pl.multiple_of(i * qw, qw), qw)]
        q = jnp.dot(xn[0:tok], w, preferred_element_type=F32)
        for h in range(group):
            v = head_rms(q[:, h * hd : (h + 1) * hd], query_gain[...] * factor)
            dst[h * tok : (h + 1) * tok] = rotate(v, cosine, sine).astype(BF16)

    def q_copy(i, slot):
        return remote(q_send.at[i], qb.at[slot], q_ss.at[i], q_rs.at[slot], sp=chip(g, i))

    def before(n):
        return lax.rem(f + fan - n, fan) if fan > 1 else 0

    def after(n):
        return lax.rem(f + 1 + n, fan) if fan > 1 else 0

    for d in range(1, fan):
        i = lax.rem(f + d, fan)
        project_q(i, q_send.at[i])
        q_copy(i, f).start()
        j = before(d)
        block_wait(g, j)
        pass_own(0, j)
        pass_own(1, j)
    project_q(f, qb.at[f])

    def forward(d, slot):
        peer = lax.rem(mt + d, n_tp)
        return remote(lat_next.at[mt], lat_next.at[slot], ln_ss.at[d], ln_rs.at[slot], tp=peer)

    if early:

        @pl.when(edge)
        def _():
            next_copy(0).wait_recv()
            for d in range(1, n_tp):
                forward(d, mt).start()
            cosine, sine = turns(chip(beside, f))
            for d in range(1, n_tp):
                forward(d, lax.rem(mt + d, n_tp)).wait_recv()
            modulate(lat_next, [inverse(lat_next[t].astype(F32)) for t in range(n_tp)])

            def project(i, dst):
                both = jnp.dot(xn[0:tok], wkv[i], preferred_element_type=F32)
                put_kv(both, dst, cosine, sine)

            for d in range(1, fan):
                i = lax.rem(f + d, fan)
                project(i, kv_send.at[1, i])
                kvn_copy(i, f).start()
            project(f, kvb.at[beside, f])

    def beside_wait(i):
        @pl.when(i != f)
        def _():
            kvn_copy(i, i).wait_recv()

        cxz_copy(0, i).wait_recv()

    def arrive(t, n):
        i = before(n)
        inner = jnp.logical_not(edge)

        @pl.when(inner & (g - t >= 0))
        def _():
            block_wait(g - t, i)
            pass_on(0, g - t, i)

        @pl.when(inner & (g + t < planes))
        def _():
            block_wait(g + t, i)
            pass_on(1, g + t, i)

    ahead = min(2, fan)
    for n in range(ahead):
        arrive(1, n)
    for n in range(1, fan):
        q_copy(f, before(n)).wait_recv()

    lift = math.log2(tok * n_sp / (4.0 * ctx * n_sp))
    contract = (((1,), (1,)), ((), ()))
    ones = jnp.ones((ONES, tok), BF16)

    def score(q, parts, buf, peak):
        best = None
        for at, n, key, _, add in parts:
            s = lax.dot_general(key(), q, contract, preferred_element_type=F32)
            if add:
                s = s + add
            buf[at : at + n] = s
            top8 = jnp.max(s.reshape(n // 8, 8, wide), axis=0)
            best = top8 if best is None else jnp.maximum(best, top8)
        peak[...] = jnp.max(best, axis=0, keepdims=True)

    def finish(i, parts, buf, peak):
        old = m_ref[i]
        new = jnp.maximum(peak[...], old)
        m_ref[i] = new
        total = None
        for at, n, _, value, _ in parts:
            e = jnp.exp2(buf[at : at + n] - new).astype(BF16)
            v = jnp.concatenate([value(), ones[:, :n]], axis=0)
            p = jnp.dot(v, e, preferred_element_type=F32)
            total = p if total is None else total + p
        acc_ref[i] = acc_ref[i] * jnp.exp2(old - new) + total

    def chunk_value(plane, c):
        return jnp.concatenate(
            [kvb[plane, c, tok + j * hd : tok + (j + 1) * hd] for j in range(tok // hd)], axis=1
        )

    def chunk_parts(plane, chunks):
        parts = []
        for k, c in enumerate(chunks):
            parts.append(
                (
                    k * tok,
                    tok,
                    lambda c=c: kvb[plane, c, 0:tok],
                    lambda c=c: chunk_value(plane, c),
                    0.0,
                )
            )
        ckey = jnp.concatenate([kvb[plane, c, 2 * tok : 2 * tok + ctx] for c in chunks], axis=0)
        cval = jnp.concatenate(
            [kvb[plane, c, 2 * tok + ctx : 2 * tok + 2 * ctx] for c in chunks], axis=0
        )
        cval = cval.astype(F32).T.astype(BF16)
        n = len(chunks) * ctx
        parts.append((len(chunks) * tok, n, lambda: ckey, lambda: cval, lift))
        return parts

    bufs = ((s0, n0), (s1, n1))

    def attend(parts, order, done):
        score(qb[order[0]], parts, *bufs[0])
        for k, i in enumerate(order):
            if k + 1 < len(order):
                score(qb[order[k + 1]], parts, *bufs[(k + 1) % 2])
            finish(i, parts, *bufs[k % 2])
            done(k, i)

    def nothing(k, i):
        pass

    all_groups = list(range(fan))

    @pl.loop(0, 2 * planes - 3)
    def _(v):
        t = lax.div(v + 1, 2)
        down = lax.rem(v, 2) == 1
        plane = jnp.where(down, g - t, g + t)
        valid = (plane >= 0) & (plane < planes)

        @pl.when(valid & edge & (v > 0))
        def _():
            @pl.when((t == 1) & early)
            def _():
                for n in range(fan):
                    beside_wait(before(n))

            @pl.when(jnp.logical_not((t == 1) & early))
            def _():
                for n in range(fan):
                    block_wait(plane, before(n))

        @pl.when(valid)
        def _():
            attend(chunk_parts(plane, all_groups), all_groups, nothing)

        @pl.when(down)
        def _():
            arrive(t + 1, 0)

        for n in range(1, fan):

            @pl.when(jnp.logical_not(down) & ((v > 0) | (n >= ahead)))
            def _():
                arrive(t + 1, n)

    def at_copy(i, slot):
        return remote(
            att_send.at[i], att_recv.at[slot], at_ss.at[i], at_rs.at[slot], sp=chip(g, i)
        )

    def give(n, i):
        a = acc_ref[i]
        a = a[:hd] * (1.0 / a[hd : hd + 1])
        heads = [a[:, h * tok : (h + 1) * tok].T.astype(BF16) for h in range(group)]
        dst = att_send.at[i] if n < fan - 1 else att_recv.at[f]
        for h in range(group):
            dst[:, h * hd : (h + 1) * hd] = heads[h]
        if n < fan - 1:
            at_copy(i, f).start()

    targets = [after(n) for n in range(fan)]

    @pl.when(edge)
    def _():
        far = jnp.where(bottom, planes - 1, 0)

        @pl.loop(0, fan - 1)
        def _(d):
            j = before(d)
            block_wait(far, j)
            attend(chunk_parts(far, [j]), all_groups, nothing)

        j = before(fan - 1)
        block_wait(far, j)
        attend(chunk_parts(far, [j]), targets, give)

    @pl.when(jnp.logical_not(edge))
    def _():
        for n in range(fan):
            give(n, targets[n])

    wait_all(gate_recv, red_sem.at[3])
    gate_all[mt] = lax.fori_loop(1, n_sp, lambda i, s: s + gate_recv[i], gate_recv[0])

    def ga_copy(d, slot):
        peer = lax.rem(mt + d, n_tp)
        return remote(gate_all.at[mt], gate_all.at[slot], ga_ss.at[d], ga_rs.at[slot], tp=peer)

    for d in range(1, n_tp):
        ga_copy(d, mt).start()
    out_load.wait()

    def out_rows(i):
        return wo[pl.ds(pl.multiple_of(i * qw, qw), qw)] if fan > 1 else wo[...]

    def project_out(t, i):
        r = pl.ds(pl.multiple_of(t * rows, rows), rows)
        p = jnp.dot(att_recv[i, r], out_rows(i), preferred_element_type=F32)
        return (psum[r] + p if fan > 1 else p).astype(BF16)

    if fan > 1:
        psum[...] = jnp.dot(att_recv[f], out_rows(f), preferred_element_type=F32)
    for n in range(1, fan - 1):
        i = before(n)
        at_copy(f, i).wait_recv()
        psum[...] += jnp.dot(att_recv[i], out_rows(i), preferred_element_type=F32)
    last = before(fan - 1)
    if fan > 1:
        at_copy(f, last).wait_recv()

    def pt_copy(d, t, slot):
        return remote(part_send.at[t], part_recv.at[slot], pt_ss.at[t], pt_rs.at[slot], tp=t)

    for d in range(1, n_tp):
        t = lax.rem(mt + d, n_tp)
        part_send[t] = project_out(t, last)
        pt_copy(d, t, mt).start()
    part_recv[mt] = project_out(mt, last)
    for d in range(1, n_tp):
        ga_copy(d, lax.rem(mt + d, n_tp)).wait_recv()
    for d in range(1, n_tp):
        t = lax.rem(mt + d, n_tp)
        pt_copy(d, t, t).wait_recv()
    mixed = part_recv[0].astype(F32)
    for t in range(1, n_tp):
        mixed = mixed + part_recv[t].astype(F32)
    inv = lax.rsqrt(jnp.mean(mixed * mixed, axis=-1, keepdims=True) + EPS)
    for t in range(n_tp):
        cols = slice(t * width, (t + 1) * width)
        out[:, cols] = (
            latent[:, cols].astype(F32)
            + gate_all[t] * (mixed[:, cols] * inv * post_gain[:, cols])
        ).astype(BF16)

    wait_all(mod_recv, red_sem.at[0])
    wait_all(gate_recv, red_sem.at[2])

    for d in range(1, n_tp):
        lat_copy(d, mt).wait_send()
        ma_copy(d, mt).wait_send()
        ga_copy(d, mt).wait_send()
        t = lax.rem(mt + d, n_tp)
        pt_copy(d, t, mt).wait_send()
    for d in range(1, fan):
        i = lax.rem(f + d, fan)
        kva_copy(i).wait_send()
        q_copy(i, f).wait_send()
        at_copy(i, f).wait_send()

    if early:

        @pl.when(send_up)
        def _():
            next_copy(0).wait_send()

        @pl.when(send_down)
        def _():
            next_copy(1).wait_send()

        @pl.when(edge)
        def _():
            for d in range(1, n_tp):
                forward(d, mt).wait_send()
            for d in range(1, fan):
                kvn_copy(lax.rem(f + d, fan), f).wait_send()

    for i in range(fan):

        @pl.when((g < planes - 1) & jnp.logical_not(send_up))
        def _():
            kvz_copy(0, g, i, chip(g, i)).wait_send()

        @pl.when((g > 0) & jnp.logical_not(send_down))
        def _():
            kvz_copy(1, g, i, n_sp + i).wait_send()

        @pl.when(send_up | send_down)
        def _():
            cxz_copy(0, i).wait_send()

    @pl.when(jnp.logical_not(edge))
    def _():
        @pl.loop(0, planes)
        def _(plane):
            @pl.when(plane != g)
            def _():
                for i in range(fan):
                    kvz_copy(0, plane, i, chip(plane, i)).wait_send()


def body(
    latent,
    condition,
    context_condition,
    context,
    w_shift,
    w_scale,
    w_gate,
    pre_gain,
    post_gain,
    query_gain,
    key_gain,
    w_query,
    w_key,
    w_value,
    w_out,
):
    n_sp = lax.axis_size("sp")
    n_tp = lax.axis_size("tp")
    hd = query_gain.shape[0]
    kv_dev = w_key.shape[1] // hd
    group = w_query.shape[1] // w_key.shape[1]
    fan = kv_dev
    planes = n_sp // fan
    rows, depth = latent.shape
    tok = rows * n_tp
    ctx = context.shape[0]
    width = w_shift.shape[1]
    sizes = (n_sp, n_tp, fan, planes, group, hd, tok, rows, ctx)
    chunk = 2 * tok + 2 * ctx
    keys = fan * (tok + ctx)
    wide = group * tok
    vmem = pl.BlockSpec(memory_space=pltpu.VMEM)
    hbm = pl.BlockSpec(memory_space=pl.ANY)
    dma = pltpu.SemaphoreType.DMA
    scratch = [
        pltpu.VMEM(w_query.shape, BF16),
        pltpu.VMEM((fan, depth, 2 * hd), BF16),
        pltpu.VMEM(w_out.shape, BF16),
        pltpu.VMEM((n_tp, rows, depth), BF16),
        pltpu.VMEM((n_tp, rows, depth), BF16),
        pltpu.VMEM((4, width), F32),
        pltpu.VMEM((n_sp, 4, width), F32),
        pltpu.VMEM((1, width), F32),
        pltpu.VMEM((n_sp, 1, width), F32),
        pltpu.VMEM((n_tp, 4, width), F32),
        pltpu.VMEM((n_tp, 1, width), F32),
        pltpu.VMEM((tok + ctx, depth), BF16),
        pltpu.VMEM((2, fan, chunk, hd), BF16),
        pltpu.VMEM((fan, wide, hd), BF16),
        pltpu.VMEM((planes, fan, chunk, hd), BF16),
        pltpu.VMEM((fan, wide, hd), BF16),
        pltpu.VMEM((fan, 1, wide), F32),
        pltpu.VMEM((fan, hd + ONES, wide), F32),
        pltpu.VMEM((keys, wide), F32),
        pltpu.VMEM((keys, wide), F32),
        pltpu.VMEM((1, wide), F32),
        pltpu.VMEM((1, wide), F32),
        pltpu.VMEM((fan, tok, group * hd), BF16),
        pltpu.VMEM((fan, tok, group * hd), BF16),
        pltpu.VMEM((tok, depth), F32),
        pltpu.VMEM((n_tp, rows, depth), BF16),
        pltpu.VMEM((n_tp, rows, depth), BF16),
        dma((2 + 2 * fan,)),
        dma((n_tp,)),
        dma((n_tp,)),
        dma((n_tp,)),
        dma((n_tp,)),
        dma((2,)),
        dma((4,)),
        dma((n_tp,)),
        dma((n_tp,)),
        dma((n_tp,)),
        dma((n_tp,)),
        dma((2, fan)),
        dma((n_sp + fan,)),
        dma((n_sp,)),
        dma((fan,)),
        dma((fan,)),
        dma((fan,)),
        dma((fan,)),
        dma((fan,)),
        dma((fan,)),
        dma((n_tp,)),
        dma((n_tp,)),
    ]
    return pl.pallas_call(
        functools.partial(kernel, sizes),
        out_shape=jax.ShapeDtypeStruct(latent.shape, BF16),
        in_specs=[vmem] * 11 + [hbm] * 4,
        out_specs=vmem,
        scratch_shapes=scratch,
        compiler_params=pltpu.CompilerParams(
            collective_id=0, has_side_effects=True, vmem_limit_bytes=60 * 1024 * 1024
        ),
    )(
        latent,
        condition.reshape(1, -1),
        context_condition.reshape(1, -1),
        context,
        w_shift,
        w_scale,
        w_gate,
        pre_gain.reshape(1, -1),
        post_gain.reshape(1, -1),
        query_gain.reshape(1, -1),
        key_gain.reshape(1, -1),
        w_query,
        w_key,
        w_value,
        w_out,
    )


def solution(mesh):
    placed = (
        P(("sp", "tp"), None),
        P("sp"),
        P("sp"),
        P("sp", None),
        P("sp", "tp"),
        P("sp", "tp"),
        P("sp", "tp"),
        P(),
        P(),
        P(),
        P(),
        P(None, "tp"),
        P(None, "tp"),
        P(None, "tp"),
        P("tp", None),
    )
    return jax.shard_map(
        body, mesh=mesh, in_specs=placed, out_specs=P(("sp", "tp"), None), check_vma=False
    )
```

time: 84.9 us -> 72.1 us (0.85)
  Pallas kernels: 82.8 us -> 70.1 us
    pallas_call x1, Pallas kernels: 82.8 us -> 70.1 us  [body(): pl.pallas_call(functools.partial(kernel, sizes), out_shape=jax.ShapeDtype...]
where the time goes in v1:
time: 72.1 us; the launch traced here: 72 us
  Pallas kernels  70.1 us (97%)
  local copies, waits for them, and re-layouts  1.88 us (3%)
    pallas_call x1, Pallas kernels, body(): pl.pallas_call(functools.partial(kernel, sizes), out_shape=jax.ShapeDtype...  70.1 us
    unnamed x1, local copies, waits for them, and re-layouts  1.88 us

profile of v1, /device:TPU:1, one launch (start us, length us, event | category | flops | bytes accessed | tf_op | source)
XLA Modules:
  0.0 72.0 jit_solution(10302390671828750676)
XLA Ops:
  0.0 70.1 %shard_map.145 = bf16[128,2048]{1,0:T(8,128)(2,1)} custom-call(bf16[128,2048]{1,0:T(8,128)(2,1)} %latent.1, bf16[1,128]{1,0:T(2,128)(2,1)} %bitcast.8, bf16[1,128]{1,0:T(2,128)(2,1)} %bitcast.9, bf16[32,2048]{1,0:T(8,128)(2,1)} %context.1, bf16[128,1024]{1,0:T(8,128)(2,1)} %w_shift.1, bf16[128,1024]{1,0:T(8,128)(2,1)} %w_scale.1, bf16[128,1024]{1,0:T(8,128)(2,1)} %w_gate.1, ...), custom_call_target="tpu_custom_call" | custom-call | tf_op jit(solution)/shard_map/pallas_call | solution.py:749
  70.1 1.9 %copy.17 = bf16[128,2048]{1,0:T(8,128)(2,1)} copy(bf16[128,2048]{1,0:T(8,128)(2,1)} %shard_map.145) | data formatting | bytes 1048576
